TPU v7x, 512 devices: a whole 4x4x16 slice. The times are simulated.
512 devices in a mesh: kv: 128 (over z, x, core), tp: 4 (over y).
Axes of the slice: x: 4, y: 4, z: 16, core: 2. Of those that a mesh axis runs over, the one named last changes fastest.
Arguments:
- tokens: bfloat16 [4, 4096], P(None, 'kv'), may hold values from -30 to 30
- norm_gain: float32 [4096], P('kv'), may hold values from 0.1 to 1.9
- query_weight: bfloat16 [4096, 2048], P('kv', 'tp'), may hold values from -0.09375 to 0.09375
- cache_keys: bfloat16 [4, 65536, 16, 128], P(None, 'kv', 'tp'), may hold values from -180 to 180
- cache_values: bfloat16 [4, 65536, 16, 128], P(None, 'kv', 'tp'), may hold values from -6 to 6
- lengths: int32 [4], replicated, may hold values from 32769 to 65536, as said below
- lambdas: float32 [16], P('tp'), may hold values from 0.3 to 0.8
- head_gain: float32 [128], replicated, may hold values from 0.1 to 1.9
- out_weight: bfloat16 [2048, 4096], P('tp', 'kv'), may hold values from -0.125 to 0.125
Outputs:
- mixed: bfloat16 [4, 4096], P(None, 'kv')
Inputs may be any that keep to these rules, and one draw needn't show every extreme that they name: `lengths`: every length is more than half of 65536; some sequence has exactly 65536.
All inputs are finite; a program needn't handle non-finite values.
Results may differ from a plain program's by a relative error of at most 0.02.
Values may be sent and summed in bfloat16 or wider, within the bound.
A program may use at most 64 MiB of HBM per device.

v0:
```python
import functools

import jax
import jax.numpy as jnp
from jax import lax
from jax.sharding import Mesh
from jax.sharding import PartitionSpec as P

D = 4096
HD = 64
VD = 128
KV = ("kv_0", "kv_1", "kv_2")


eps = 1e-06
NEG = -1e30


def one_axis_at_a_time(shard, axes):
    return functools.reduce(lax.psum, axes, shard)


def collected_together(shard, axis):
    leaves = jax.tree.leaves(shard)
    turns = sorted(range(len(leaves)), key=lambda k: -leaves[k].size)
    width = (1, *leaves[turns[0]].shape)[-1]
    lines = [
        jnp.pad(leaves[k].reshape(-1), (0, -leaves[k].size % width)).reshape(-1, width)
        for k in turns
    ]
    both, at, found = (lax.all_gather(jnp.concatenate(lines), axis), 0, {})
    for k, line in zip(turns, lines):
        share = both[:, at : at + len(line)].reshape(len(both), -1)
        found[k] = share[:, : leaves[k].size].reshape(-1, *leaves[k].shape)
        at += len(line)
    numbers = iter(range(len(leaves)))
    return jax.tree.map(lambda _: found[next(numbers)], shard)


def merged_by_axis(shard, axes, combine):
    for axis in axes:
        pieces = collected_together(shard, axis)
        shard = jax.tree.map(lambda part: part[0], pieces)
        for k in range(1, lax.axis_size(axis)):
            shard = combine(shard, jax.tree.map(lambda part: part[k], pieces))
    return shard


def sent_to_all(shard, axis):
    devices = lax.axis_size(axis)
    return lax.all_to_all(
        jnp.broadcast_to(shard[None], (devices, *shard.shape)), axis, 0, 0, tiled=True
    )


def over_copies(shard, axis):
    return sent_to_all(shard, axis).astype(jnp.float32).sum(axis=0)


def combine_parts(first, second):
    peak = jnp.maximum(first[0], second[0])
    factor_one = jnp.exp(first[0] - peak)
    second_factor_term = jnp.exp(second[0] - peak)
    return (
        peak,
        first[1] * factor_one + second[1] * second_factor_term,
        first[2] * factor_one[..., None] + second[2] * second_factor_term[..., None],
    )


def body(
    tokens,
    norm_gain,
    query_weight,
    cache_keys,
    cache_values,
    lengths,
    lambdas,
    head_gain,
    out_weight,
):
    seqs = tokens.shape[0]
    span = cache_keys.shape[1]
    local_heads = cache_keys.shape[2]
    floats = tokens.astype(jnp.float32)
    squares = jnp.sum(floats * floats, axis=1)
    scaled_logits = (floats * norm_gain).astype(jnp.bfloat16)
    partial_value = jnp.dot(scaled_logits, query_weight, preferred_element_type=jnp.float32)
    total_squares, projected = (
        one_axis_at_a_time(squares, KV),
        one_axis_at_a_time(partial_value, KV),
    )
    inverse = lax.rsqrt(total_squares / D + eps)
    query = (
        (projected * inverse[:, None] * 0.125)
        .astype(jnp.bfloat16)
        .reshape(seqs, local_heads, 2, HD)
    )
    keys = cache_keys.reshape(seqs, span, local_heads, 2, HD)
    score_matrix = jnp.einsum("bhmd,bphmd->bhmp", query, keys, preferred_element_type=jnp.float32)
    position_indices = lax.axis_index(KV) * span + jnp.arange(span, dtype=jnp.int32)
    valid = (position_indices[None, :] < lengths[:, None])[:, None, None, :]
    score_matrix = jnp.where(valid, score_matrix, NEG)
    peak = jnp.max(score_matrix, axis=-1)
    weights = jnp.where(valid, jnp.exp(score_matrix - peak[..., None]), 0.0)
    mass = jnp.sum(weights, axis=-1)
    summed = jnp.einsum(
        "bhmp,bphv->bhmv",
        weights.astype(jnp.bfloat16),
        cache_values,
        preferred_element_type=jnp.float32,
    )
    scales = lambdas[None, :, None]
    whole_peak, whole_mass, whole_sum = merged_by_axis((peak, mass, summed), KV, combine_parts)
    attended = (
        whole_sum[:, :, 0] / whole_mass[:, :, 0, None]
        - scales * whole_sum[:, :, 1] / whole_mass[:, :, 1, None]
    )
    normed = (
        attended
        * lax.rsqrt(jnp.mean(attended * attended, axis=-1, keepdims=True) + eps)
        * head_gain
        * 0.8
    )
    normed = normed.astype(jnp.bfloat16).reshape(seqs, local_heads * VD)
    part = jnp.dot(normed, out_weight, preferred_element_type=jnp.float32).astype(jnp.bfloat16)
    return over_copies(part, "tp").astype(jnp.float32).astype(jnp.bfloat16)


def solution(mesh):
    split = Mesh(mesh.devices.reshape(16, 4, 2, mesh.shape["tp"]), ("kv_0", "kv_1", "kv_2", "tp"))
    in_specs = (
        P(None, KV),
        P(KV),
        P(KV, "tp"),
        P(None, KV, "tp", None),
        P(None, KV, "tp", None),
        P(),
        P("tp"),
        P(),
        P("tp", KV),
    )
    out_specs = P(None, KV)
    return jax.shard_map(body, mesh=split, in_specs=in_specs, out_specs=out_specs, check_vma=False)
```

profile of v0, /device:TPU:1, one launch (start us, length us, event | category | flops | bytes accessed | tf_op | source)
XLA Modules:
  0.0 113.3 jit_solution(6306658680171734619)
XLA Ops:
  0.0 0.0 copy-start
  0.0 0.9 fusion.68
  0.9 0.9 fusion.69
  1.9 31.2 %all-reduce.6 = (f32[4,512]{1,0:T(4,128)S(1)}, f32[4]{0:T(128)S(1)}) all-reduce(f32[4,512]{1,0:T(4,128)S(1)} %fusion.69, f32[4]{0:T(128)S(1)} %fusion.68), channel_id=1, replica_groups=mesh['kv_0'=16,'kv_1'=4,'kv_2'=2,'tp'=4] {'kv_0'}, use_global_device_ids=true, to_apply=%region_0.0 | all-reduce | flops 2052 | bytes 16416 | tf_op jit(solution)/shard_map/psum | solution.py:20
  33.1 8.7 %all-reduce.7 = (f32[4,512]{1,0:T(4,128)S(1)}, f32[4]{0:T(128)S(1)}) all-reduce(f32[4,512]{1,0:T(4,128)S(1)} %get-tuple-element.11, f32[4]{0:T(128)S(1)} %get-tuple-element.12), channel_id=1, replica_groups=mesh['kv_0'=16,'kv_1'=4,'kv_2'=2,'tp'=4] {'kv_1'}, use_global_device_ids=true, to_apply=%region_1.0 | all-reduce | flops 2052 | bytes 16416 | tf_op jit(solution)/shard_map/psum | solution.py:20
  41.8 12.0 %all-reduce.8 = (f32[4,512]{1,0:T(4,128)S(1)}, f32[4]{0:T(128)S(1)}) all-reduce(f32[4,512]{1,0:T(4,128)S(1)} %get-tuple-element.13, f32[4]{0:T(128)S(1)} %get-tuple-element.14), channel_id=1, replica_groups=mesh['kv_0'=16,'kv_1'=4,'kv_2'=2,'tp'=4] {'kv_2'}, use_global_device_ids=true, to_apply=%region_2.0 | all-reduce | flops 2052 | bytes 16416 | tf_op jit(solution)/shard_map/psum | solution.py:20
  53.8 0.1 multiply_convert_fusion
  53.8 0.1 reshape.1493
  53.9 4.3 %copy.18 = bf16[4,512,4,128]{1,3,2,0:T(8,128)(2,1)} copy(bf16[4,512,4,128]{3,2,1,0:T(4,128)(2,1)} %param.12) | data formatting | bytes 4194304 | tf_op args[3]
  58.2 0.0 copy-start.2
  58.2 2.0 %fusion.160 = f32[4,4,2,1,512]{4,3,2,1,0:T(1,128)S(1)} fusion(bf16[4,4,2,64,1]{3,4,2,1,0:T(2,128)(2,1)S(1)} %reshape.1493, bf16[4,512,4,2,64]{1,4,3,2,0:T(8,128)(2,1)} %bitcast.695), kind=kOutput, calls=%fused_computation.280 | convolution fusion | flops 2097152 | bytes 2166784 | tf_op jit(solution)/shard_map/bhmd,bphmd->bhmp/dot_general | solution.py:100
  60.2 0.0 copy-done.2
  60.2 0.1 broadcast_compare_fusion
  60.2 0.1 fusion.2
  60.4 0.2 fusion.142
  60.6 0.0 copy-start.1
  60.6 0.1 reshape.1464
  60.7 0.0 copy-done
  60.7 0.0 copy-start.3
  60.7 0.0 copy-start.4
  60.7 0.4 fusion
  61.2 0.1 reshape.1466
  61.3 21.0 %all-gather.3 = f32[16,34,128]{2,1,0:T(8,128)S(1)} all-gather(f32[1,34,128]{2,1,0:T(8,128)S(1)} %maximum_bitcast_fusion), channel_id=2, replica_groups=mesh['kv_0'=16,'kv_1'=4,'kv_2'=2,'tp'=4] {'kv_0'}, dimensions={0}, use_global_device_ids=true | all-gather | bytes 295936 | tf_op jit(solution)/shard_map/all_gather | solution.py:31
  82.4 0.1 fusion.73
  82.5 0.2 fusion.14
  82.7 9.2 %all-gather.4 = f32[4,34,128]{2,1,0:T(8,128)S(1)} all-gather(f32[1,34,128]{2,1,0:T(8,128)S(1)} %maximum_bitcast_fusion.1), channel_id=3, replica_groups=mesh['kv_0'=16,'kv_1'=4,'kv_2'=2,'tp'=4] {'kv_1'}, dimensions={0}, use_global_device_ids=true | all-gather | bytes 87040 | tf_op jit(solution)/shard_map/all_gather | solution.py:31
  91.9 0.1 fusion.5
  92.0 11.4 %all-gather.5 = f32[2,34,128]{2,1,0:T(8,128)S(1)} all-gather(f32[1,34,128]{2,1,0:T(8,128)S(1)} %maximum_bitcast_fusion.2), channel_id=4, replica_groups=mesh['kv_0'=16,'kv_1'=4,'kv_2'=2,'tp'=4] {'kv_2'}, dimensions={0}, use_global_device_ids=true | all-gather | bytes 52224 | tf_op jit(solution)/shard_map/all_gather | solution.py:31
  103.4 0.1 squeeze.274
  103.5 0.1 squeeze.273
  103.6 0.1 squeeze.269
  103.7 0.1 squeeze.270
  103.9 0.1 multiply_add_fusion
  104.0 0.1 slice_reduce_fusion.1
  104.2 0.0 copy-done.1
  104.2 0.2 broadcast_bitcast_fusion.2
  104.4 0.1 broadcast_bitcast_fusion
  104.4 0.0 copy-done.3
  104.4 0.1 broadcast_bitcast_fusion.3
  104.5 0.0 copy-done.4
  104.5 0.1 convolution_convert_fusion
  104.6 8.1 %all_to_all.5 = bf16[4,4,32]{2,1,0:T(4,128)(2,1)S(1)} all-to-all(bf16[4,4,32]{2,1,0:T(4,128)(2,1)S(1)} %broadcast_in_dim.23), channel_id=1, replica_groups=mesh['kv_0'=16,'kv_1'=4,'kv_2'=2,'tp'=4] {'tp'}, dimensions={0} | all-to-all | bytes 2048 | tf_op jit(solution)/shard_map/all_to_all | solution.py:51
  112.8 0.6 reduce_sum.42
  (22 shorter events, 0.2 us)
Async XLA Ops:
  0.0 60.7 %copy-start = (bf16[4,512,4,128]{3,2,1,0:T(4,128)(2,1)S(1)}, bf16[4,512,4,128]{3,2,1,0:T(4,128)(2,1)}, u32[]{:S(2)}) copy-start(bf16[4,512,4,128]{3,2,1,0:T(4,128)(2,1)} %param.13) | copy-start | bytes 6291460
  58.2 2.0 %copy-start.2 = (s32[4]{0:T(128)S(1)}, s32[4]{0:T(128)}, u32[]{:S(2)}) copy-start(s32[4]{0:T(128)} %param.14) | copy-start | bytes 52
  60.6 43.6 %copy-start.1 = (f32[4]{0:T(128)S(1)}, f32[4]{0:T(128)}, u32[]{:S(2)}) copy-start(f32[4]{0:T(128)} %param.15) | copy-start | bytes 52
  60.7 43.7 %copy-start.3 = (f32[128]{0:T(128)S(1)}, f32[128]{0:T(128)}, u32[]{:S(2)}) copy-start(f32[128]{0:T(128)} %param.16) | copy-start | bytes 1540
  60.7 43.8 %copy-start.4 = (bf16[512,32]{0,1:T(8,128)(2,1)S(1)}, bf16[512,32]{0,1:T(8,128)(2,1)}, u32[]{:S(2)}) copy-start(bf16[512,32]{0,1:T(8,128)(2,1)} %param.17) | copy-start | bytes 98308
where the time goes:
time: 114 us; the launch traced here: 113 us
  blocking collectives  102 us (89%)
  local copies, waits for them, and re-layouts  5.34 us (5%)
  matrix products  3.46 us (3%)
  other arithmetic  2.79 us (2%)
    psum x3, blocking collectives, one_axis_at_a_time(): return functools.reduce(lax.psum, axes, shard)  51.9 us
    all_gather x3, blocking collectives, collected_together(): both, at, found = (lax.all_gather(jnp.concatenate(lines), axis), 0, {})  41.6 us
    all_to_all x1, blocking collectives, sent_to_all(): lax.all_to_all(jnp.broadcast_to(shard[None], (devices, *shard.shape)), ax...  8.12 us
    unnamed x12, local copies, waits for them, and re-layouts  4.37 us

commit v1 on v0

v1 whole, which is shorter than its diff:
```python
import functools

import jax
import jax.numpy as jnp
from jax import lax
from jax.experimental import pallas as pl
from jax.experimental.pallas import tpu as pltpu
from jax.sharding import PartitionSpec as P

MESH = pl.DeviceIdType.MESH
D = 4096
HD = 64
NEAR = 8
FAR = 16
GROUPS = 4
SEQS = 4
HEADS = 4
eps = 1e-06
NEG = -1e30
F32 = jnp.float32
BF16 = jnp.bfloat16


def kernel(
    tokens_hbm, gain_hbm, wq_hbm, keys_hbm, values_hbm, lengths_hbm, lambdas_hbm, hgain_hbm, wo_hbm,
    out_ref,
    tokens, gain, wq, keys, values, lengths, lambdas, hgain, wo,
    a_send, a_near, a_far, qbuf, c_send, c_near, c_far, nbuf, pbuf,
    small_sem, kv_sem, send_sem, a_near_sem, a_far_sem, q_sem, c_near_sem, c_far_sem, n_sem, p_sem,
):
    kv = lax.axis_index("kv")
    tp = lax.axis_index("tp")
    near = lax.rem(kv, NEAR)
    far = kv // NEAR
    core = lax.rem(near, 2)
    chip = near // 2
    span = keys.shape[1] // HEADS

    def near_id(d):
        return (far * NEAR + lax.rem(near + d, NEAR), tp)

    def far_id(d):
        return (lax.rem(far + d, FAR) * NEAR + near, tp)

    def group_id(d):
        return (kv, lax.rem(tp + d, GROUPS))

    barrier = pltpu.get_barrier_semaphore()
    for d in range(1, FAR):
        pl.semaphore_signal(barrier, inc=1, device_id=far_id(d), device_id_type=MESH)
    for d in range(1, NEAR):
        pl.semaphore_signal(barrier, inc=1, device_id=near_id(d), device_id_type=MESH)
    for d in range(1, GROUPS):
        pl.semaphore_signal(barrier, inc=1, device_id=group_id(d), device_id_type=MESH)

    small = [
        pltpu.make_async_copy(src, dst, small_sem.at[k])
        for k, (src, dst) in enumerate(
            [
                (tokens_hbm, tokens), (gain_hbm, gain), (wq_hbm, wq), (lengths_hbm, lengths),
                (lambdas_hbm, lambdas), (hgain_hbm, hgain), (wo_hbm, wo),
            ]
        )
    ]
    for copy in small:
        copy.start()
    cache = []
    for s in range(SEQS):
        cache.append(pltpu.make_async_copy(keys_hbm.at[s], keys.at[s], kv_sem.at[s]))
        cache.append(pltpu.make_async_copy(values_hbm.at[s], values.at[s], kv_sem.at[SEQS + s]))
    for copy in cache:
        copy.start()
    for copy in small[:3]:
        copy.wait()

    floats = tokens[...].astype(F32)
    squares = jnp.sum(floats * floats, axis=1, keepdims=True)
    scaled = (floats * gain[...]).astype(BF16)
    partial = jnp.dot(scaled, wq[...], preferred_element_type=F32)
    for s in range(SEQS):
        for half in range(2):
            for r in range(2):
                c = (2 * half + r) * 128
                a_send[2 * s + half, r : r + 1, :] = partial[s : s + 1, c : c + 128]
            a_send[2 * s + half, 2:3, :] = jnp.broadcast_to(squares[s : s + 1, :], (1, 128))

    pl.semaphore_wait(barrier, FAR + NEAR + GROUPS - 3)

    sends = []

    def send(src, dst, recv, device):
        copy = pltpu.make_async_remote_copy(
            src_ref=src, dst_ref=dst, send_sem=send_sem.at[len(sends)], recv_sem=recv,
            device_id=device, device_id_type=MESH,
        )
        copy.start()
        sends.append(copy)

    def landed(buf, slot, sem):
        pltpu.make_async_copy(buf.at[slot], buf.at[slot], sem.at[slot]).wait()

    for d in range(1, NEAR):
        j = lax.rem(near + d, NEAR)
        send(a_send.at[j], a_near.at[near], a_near_sem.at[near], near_id(d))
    a_near[near] = a_send[near]
    for d in range(1, NEAR):
        landed(a_near, lax.rem(near + d, NEAR), a_near_sem)
    a_far[far] = jnp.sum(a_near[...], axis=0)
    for d in (8, 7, 9, 6, 10, 5, 11, 4, 12, 3, 13, 2, 14, 1, 15):
        send(a_far.at[far], a_far.at[far], a_far_sem.at[far], far_id(d))
    for d in range(1, FAR):
        landed(a_far, lax.rem(far + d, FAR), a_far_sem)
    total = jnp.sum(a_far[...], axis=0)
    inverse = lax.rsqrt(total[2:3, :] / D + eps)
    qbuf[near] = (total[0:2, :] * inverse * 0.125).astype(BF16).astype(F32)
    for d in (4, 5, 3, 2, 6, 7, 1):
        send(qbuf.at[near], qbuf.at[near], q_sem.at[near], near_id(d))
    for copy in small[3:]:
        copy.wait()

    width = keys.shape[1]
    row = lax.broadcasted_iota(jnp.int32, (2 * HEADS, width), 0)
    column = lax.broadcasted_iota(jnp.int32, (2 * HEADS, width), 1)
    own_head = (column % HEADS) == (row // 2)
    lane8 = lax.broadcasted_iota(jnp.int32, (2 * HEADS, 128), 1)
    row8 = lax.broadcasted_iota(jnp.int32, (2 * HEADS, 128), 0)
    map_lanes = (lane8 // HD) == (row8 % 2)

    for turn in (0, 1, 3, 2):
        s = lax.rem(chip + turn, SEQS)
        for half in range(2):
            if turn:
                landed(qbuf, 2 * s + half, q_sem)
        if not turn:
            landed(qbuf, 2 * s + 1 - core, q_sem)
        heads = []
        for h in range(HEADS):
            line = qbuf[2 * s + h // 2, h % 2 : h % 2 + 1, :]
            heads += [line, line]
        q8 = jnp.where(map_lanes, jnp.concatenate(heads, axis=0), 0.0).astype(BF16)
        pltpu.make_async_copy(keys_hbm.at[s], keys.at[s], kv_sem.at[s]).wait()
        scores = lax.dot_general(
            q8, keys[s], (((1,), (1,)), ((), ())), preferred_element_type=F32
        )
        valid = own_head & (column < (lengths[s] - kv * span) * HEADS)
        scores = jnp.where(valid, scores, NEG)
        peak = jnp.max(scores, axis=1, keepdims=True)
        weights = jnp.where(valid, jnp.exp(scores - peak), 0.0)
        mass = jnp.sum(weights, axis=1, keepdims=True)
        pltpu.make_async_copy(values_hbm.at[s], values.at[s], kv_sem.at[SEQS + s]).wait()
        summed = jnp.dot(weights.astype(BF16), values[s], preferred_element_type=F32)
        stats = jnp.sum(
            jnp.where(lane8 == row8, mass, 0.0) + jnp.where(lane8 == row8 + 8, peak, 0.0),
            axis=0, keepdims=True,
        )
        for half in range(2):
            c_send[2 * s + half, 0:4, :] = summed[4 * half : 4 * half + 4, :]
            c_send[2 * s + half, 4:5, :] = stats
        if turn:
            for half in range(2):
                send(
                    c_send.at[2 * s + half], c_near.at[near], c_near_sem.at[near],
                    (far * NEAR + 2 * s + half, tp),
                )
        else:
            send(
                c_send.at[2 * s + 1 - core], c_near.at[near], c_near_sem.at[near],
                (far * NEAR + 2 * s + 1 - core, tp),
            )
            c_near[near] = c_send[near]

    def merged(box, first):
        count = box.shape[0]
        lane = lax.broadcasted_iota(jnp.int32, (count, 4, 128), 2)
        line = lax.broadcasted_iota(jnp.int32, (count, 4, 128), 1)
        both = box[:, 4:5, :]
        masses = jnp.sum(jnp.where(lane == line + first, both, 0.0), axis=2, keepdims=True)
        peaks = jnp.sum(jnp.where(lane == line + first + 8, both, 0.0), axis=2, keepdims=True)
        top = jnp.max(peaks, axis=0, keepdims=True)
        factor = jnp.exp(peaks - top)
        return top[0], jnp.sum(masses * factor, axis=0), jnp.sum(box[:, 0:4, :] * factor, axis=0)

    for d in range(1, NEAR):
        landed(c_near, lax.rem(near + d, NEAR), c_near_sem)
    peak, mass, summed = merged(c_near[...], 4 * core)
    lane4 = lax.broadcasted_iota(jnp.int32, (4, 128), 1)
    row4 = lax.broadcasted_iota(jnp.int32, (4, 128), 0)
    stats = jnp.sum(
        jnp.where(lane4 == row4, mass, 0.0) + jnp.where(lane4 == row4 + 8, peak, 0.0),
        axis=0, keepdims=True,
    )
    c_far[far, 0:4, :] = summed
    c_far[far, 4:5, :] = stats
    for d in (8, 7, 9, 6, 10, 5, 11, 4, 12, 3, 13, 2, 14, 1, 15):
        send(c_far.at[far], c_far.at[far], c_far_sem.at[far], far_id(d))
    for d in range(1, FAR):
        landed(c_far, lax.rem(far + d, FAR), c_far_sem)
    peak, mass, summed = merged(c_far[...], 0)
    ratio = summed / mass
    lines = []
    for h in range(2):
        attended = ratio[2 * h : 2 * h + 1, :] - lambdas[2 * core + h] * ratio[2 * h + 1 : 2 * h + 2, :]
        mean = jnp.mean(attended * attended, axis=1, keepdims=True)
        lines.append(attended * lax.rsqrt(mean + eps) * hgain[...] * 0.8)
    nbuf[near] = jnp.concatenate(lines, axis=0).astype(BF16).astype(F32)
    for d in (4, 5, 3, 2, 6, 7, 1):
        send(nbuf.at[near], nbuf.at[near], n_sem.at[near], near_id(d))
    for d in range(1, NEAR):
        landed(nbuf, lax.rem(near + d, NEAR), n_sem)
    part = jnp.zeros((SEQS, 32), F32)
    for h in range(HEADS):
        head = jnp.concatenate(
            [nbuf[2 * s + h // 2, h % 2 : h % 2 + 1, :] for s in range(SEQS)], axis=0
        ).astype(BF16)
        part += lax.dot_general(
            head, wo[:, 128 * h : 128 * (h + 1)], (((1,), (1,)), ((), ())),
            preferred_element_type=F32,
        )
    part = part.astype(BF16).astype(F32)
    pbuf[tp] = jnp.concatenate([part, jnp.zeros((SEQS, 96), F32)], axis=1)
    for d in (2, 1, 3):
        send(pbuf.at[tp], pbuf.at[tp], p_sem.at[tp], group_id(d))
    for d in range(1, GROUPS):
        landed(pbuf, lax.rem(tp + d, GROUPS), p_sem)
    out_ref[...] = jnp.sum(pbuf[...], axis=0)[:, 0:32].astype(BF16)
    for copy in sends:
        copy.wait_send()


def body(tokens, norm_gain, query_weight, cache_keys, cache_values, lengths, lambdas, head_gain, out_weight):
    seqs, span, heads, size = cache_keys.shape
    hbm = pl.BlockSpec(memory_space=pltpu.HBM)
    n_sends = 7 + 15 + 7 + 7 + 15 + 7 + 3
    return pl.pallas_call(
        kernel,
        name="decode",
        out_shape=jax.ShapeDtypeStruct((seqs, 32), BF16),
        in_specs=[hbm] * 9,
        out_specs=pl.BlockSpec(memory_space=pltpu.VMEM),
        scratch_shapes=[
            pltpu.VMEM((seqs, 32), BF16),
            pltpu.VMEM((1, 32), F32),
            pltpu.VMEM((32, 512), BF16),
            pltpu.VMEM((seqs, span * heads, size), BF16),
            pltpu.VMEM((seqs, span * heads, size), BF16),
            pltpu.SMEM((seqs,), jnp.int32),
            pltpu.SMEM((heads,), F32),
            pltpu.VMEM((1, 128), F32),
            pltpu.VMEM((32, 512), BF16),
            pltpu.VMEM((NEAR, 3, 128), F32),
            pltpu.VMEM((NEAR, 3, 128), F32),
            pltpu.VMEM((FAR, 3, 128), F32),
            pltpu.VMEM((NEAR, 2, 128), F32),
            pltpu.VMEM((NEAR, 5, 128), F32),
            pltpu.VMEM((NEAR, 5, 128), F32),
            pltpu.VMEM((FAR, 5, 128), F32),
            pltpu.VMEM((NEAR, 2, 128), F32),
            pltpu.VMEM((GROUPS, SEQS, 128), F32),
            pltpu.SemaphoreType.DMA((7,)),
            pltpu.SemaphoreType.DMA((2 * SEQS,)),
            pltpu.SemaphoreType.DMA((n_sends,)),
            pltpu.SemaphoreType.DMA((NEAR,)),
            pltpu.SemaphoreType.DMA((FAR,)),
            pltpu.SemaphoreType.DMA((NEAR,)),
            pltpu.SemaphoreType.DMA((NEAR,)),
            pltpu.SemaphoreType.DMA((FAR,)),
            pltpu.SemaphoreType.DMA((NEAR,)),
            pltpu.SemaphoreType.DMA((GROUPS,)),
        ],
        compiler_params=pltpu.CompilerParams(
            collective_id=0, has_side_effects=True
        ),
    )(
        tokens,
        norm_gain.reshape(1, 32),
        query_weight,
        cache_keys.reshape(seqs, span * heads, size),
        cache_values.reshape(seqs, span * heads, size),
        lengths,
        lambdas,
        head_gain.reshape(1, 128),
        out_weight.T,
    )


def solution(mesh):
    in_specs = (
        P(None, "kv"), P("kv"), P("kv", "tp"), P(None, "kv", "tp", None), P(None, "kv", "tp", None),
        P(), P("tp"), P(), P("tp", "kv"),
    )
    return jax.shard_map(body, mesh=mesh, in_specs=in_specs, out_specs=P(None, "kv"), check_vma=False)
```

time: 114 us -> 53.2 us (0.47)
  blocking collectives: 102 us -> 0 us
  Pallas kernels: 0 us -> 51.9 us
  local copies, waits for them, and re-layouts: 5.34 us -> 1.24 us
  matrix products: 3.46 us -> 0 us
  other arithmetic: 2.79 us -> 0 us
    psum x3 -> x0, blocking collectives: 51.9 us -> none  [one_axis_at_a_time(): return functools.reduce(lax.psum, axes, shard)]
    pallas_call x0 -> x1, Pallas kernels: none -> 51.9 us  [body(): pl.pallas_call(kernel, name='decode', out_shape=jax.ShapeDtypeStruct((seq...]
    all_gather x3 -> x0, blocking collectives: 41.6 us -> none  [collected_together(): both, at, found = (lax.all_gather(jnp.concatenate(lines), axis), 0, {})]
    all_to_all x1 -> x0, blocking collectives: 8.12 us -> none  [sent_to_all(): lax.all_to_all(jnp.broadcast_to(shard[None], (devices, *shard.shape)), ax...]
    dot_general x4 -> x0, matrix products: 3.46 us -> none  [the longest x1 1.97 us: body(): jnp.einsum('bhmd,bphmd->bhmp', query, keys, preferred_element_type=jnp.fl...]
    unnamed x12 -> x1, local copies, waits for them, and re-layouts: 4.37 us -> 1.24 us
    reduce_sum x3 -> x0, other arithmetic: 1.73 us -> none  [the longest x1 0.94 us: body(): squares = jnp.sum(floats * floats, axis=1)]
where the time goes in v1:
time: 53.2 us; the launch traced here: 53.1 us
  Pallas kernels  51.9 us (98%)
  local copies, waits for them, and re-layouts  1.24 us (2%)
    pallas_call x1, Pallas kernels, body(): pl.pallas_call(kernel, name='decode', out_shape=jax.ShapeDtypeStruct((seq...  51.9 us
    unnamed x1, local copies, waits for them, and re-layouts  1.24 us

profile of v1, /device:TPU:1, one launch (start us, length us, event | category | flops | bytes accessed | tf_op | source)
XLA Modules:
  0.0 53.1 jit_solution(16361809011446736934)
XLA Ops:
  0.0 51.9 %decode.1 = bf16[4,32]{1,0:T(4,128)(2,1)} custom-call(bf16[4,32]{1,0:T(4,128)(2,1)} %tokens_hbm.1, f32[1,32]{1,0:T(1,128)} %bitcast.8, bf16[32,512]{1,0:T(8,128)(2,1)} %wq_hbm.1, bf16[4,2048,128]{2,1,0:T(8,128)(2,1)} %bitcast.5, bf16[4,2048,128]{2,1,0:T(8,128)(2,1)} %bitcast.6, s32[4]{0:T(128)} %lengths_hbm.1, f32[4]{0:T(128)} %lambdas_hbm.1, ...), custom_call_target="tpu_custom_call" | custom-call | tf_op jit(solution)/shard_map/decode/pallas_call | solution.py:234
  51.9 1.2 %copy.11 = bf16[4,32]{1,0:T(4,128)(2,1)} copy(bf16[4,32]{1,0:T(4,128)(2,1)} %decode.1) | data formatting | bytes 512

commit v2 on v1

--- a/solution.py
+++ b/solution.py
@@ -26,7 +26,7 @@
     out_ref,
     tokens, gain, wq, keys, values, lengths, lambdas, hgain, wo,
     a_send, a_near, a_far, qbuf, c_send, c_near, c_far, nbuf, pbuf,
-    small_sem, kv_sem, send_sem, a_near_sem, a_far_sem, q_sem, c_near_sem, c_far_sem, n_sem, p_sem,
+    small_sem, kv_sem, send_sem, recv_sem, q_sem, known_sem,
 ):
     kv = lax.axis_index("kv")
     tp = lax.axis_index("tp")
@@ -46,11 +46,11 @@
         return (kv, lax.rem(tp + d, GROUPS))
 
     barrier = pltpu.get_barrier_semaphore()
-    for d in range(1, FAR):
+    for d in (2, 14, 1, 15):
         pl.semaphore_signal(barrier, inc=1, device_id=far_id(d), device_id_type=MESH)
-    for d in range(1, NEAR):
+    for d in (4, 5, 3, 2, 6, 7, 1):
         pl.semaphore_signal(barrier, inc=1, device_id=near_id(d), device_id_type=MESH)
-    for d in range(1, GROUPS):
+    for d in (2, 1, 3):
         pl.semaphore_signal(barrier, inc=1, device_id=group_id(d), device_id_type=MESH)
 
     small = [
@@ -84,37 +84,38 @@
                 a_send[2 * s + half, r : r + 1, :] = partial[s : s + 1, c : c + 128]
             a_send[2 * s + half, 2:3, :] = jnp.broadcast_to(squares[s : s + 1, :], (1, 128))
 
-    pl.semaphore_wait(barrier, FAR + NEAR + GROUPS - 3)
-
-    sends = []
-
-    def send(src, dst, recv, device):
-        copy = pltpu.make_async_remote_copy(
-            src_ref=src, dst_ref=dst, send_sem=send_sem.at[len(sends)], recv_sem=recv,
+    pl.semaphore_wait(barrier, 4 + NEAR - 1 + GROUPS - 1)
+
+    def send(phase, src, dst, recv, device):
+        pltpu.make_async_remote_copy(
+            src_ref=src, dst_ref=dst, send_sem=send_sem.at[phase], recv_sem=recv,
             device_id=device, device_id_type=MESH,
-        )
-        copy.start()
-        sends.append(copy)
-
-    def landed(buf, slot, sem):
-        pltpu.make_async_copy(buf.at[slot], buf.at[slot], sem.at[slot]).wait()
-
-    for d in range(1, NEAR):
+        ).start()
+
+    def arrived(buf, count, sem):
+        view = buf.at[pl.ds(0, count)]
+        pltpu.make_async_copy(view, view, sem).wait()
+
+    for d in (4, 5, 3, 2, 6, 7, 1):
         j = lax.rem(near + d, NEAR)
-        send(a_send.at[j], a_near.at[near], a_near_sem.at[near], near_id(d))
+        send(0, a_send.at[j], a_near.at[near], recv_sem.at[0], near_id(d))
+    for d, sem in ((2, known_sem.at[0]), (4, known_sem.at[1])):
+        for e in (d, FAR - d):
+            pl.semaphore_signal(sem, inc=1, device_id=far_id(e), device_id_type=MESH)
+        if d == 2:
+            pl.semaphore_wait(sem, 2)
     a_near[near] = a_send[near]
-    for d in range(1, NEAR):
-        landed(a_near, lax.rem(near + d, NEAR), a_near_sem)
+    arrived(a_near, NEAR - 1, recv_sem.at[0])
     a_far[far] = jnp.sum(a_near[...], axis=0)
+    pl.semaphore_wait(known_sem.at[1], 2)
     for d in (8, 7, 9, 6, 10, 5, 11, 4, 12, 3, 13, 2, 14, 1, 15):
-        send(a_far.at[far], a_far.at[far], a_far_sem.at[far], far_id(d))
-    for d in range(1, FAR):
-        landed(a_far, lax.rem(far + d, FAR), a_far_sem)
+        send(1, a_far.at[far], a_far.at[far], recv_sem.at[1], far_id(d))
+    arrived(a_far, FAR - 1, recv_sem.at[1])
     total = jnp.sum(a_far[...], axis=0)
     inverse = lax.rsqrt(total[2:3, :] / D + eps)
     qbuf[near] = (total[0:2, :] * inverse * 0.125).astype(BF16).astype(F32)
     for d in (4, 5, 3, 2, 6, 7, 1):
-        send(qbuf.at[near], qbuf.at[near], q_sem.at[near], near_id(d))
+        send(2, qbuf.at[near], qbuf.at[near], q_sem.at[chip], near_id(d))
     for copy in small[3:]:
         copy.wait()
 
@@ -128,11 +129,7 @@
 
     for turn in (0, 1, 3, 2):
         s = lax.rem(chip + turn, SEQS)
-        for half in range(2):
-            if turn:
-                landed(qbuf, 2 * s + half, q_sem)
-        if not turn:
-            landed(qbuf, 2 * s + 1 - core, q_sem)
+        arrived(qbuf, 2 if turn else 1, q_sem.at[s])
         heads = []
         for h in range(HEADS):
             line = qbuf[2 * s + h // 2, h % 2 : h % 2 + 1, :]
@@ -159,12 +156,12 @@
         if turn:
             for half in range(2):
                 send(
-                    c_send.at[2 * s + half], c_near.at[near], c_near_sem.at[near],
+                    3, c_send.at[2 * s + half], c_near.at[near], recv_sem.at[2],
                     (far * NEAR + 2 * s + half, tp),
                 )
         else:
             send(
-                c_send.at[2 * s + 1 - core], c_near.at[near], c_near_sem.at[near],
+                3, c_send.at[2 * s + 1 - core], c_near.at[near], recv_sem.at[2],
                 (far * NEAR + 2 * s + 1 - core, tp),
             )
             c_near[near] = c_send[near]
@@ -180,8 +177,7 @@
         factor = jnp.exp(peaks - top)
         return top[0], jnp.sum(masses * factor, axis=0), jnp.sum(box[:, 0:4, :] * factor, axis=0)
 
-    for d in range(1, NEAR):
-        landed(c_near, lax.rem(near + d, NEAR), c_near_sem)
+    arrived(c_near, NEAR - 1, recv_sem.at[2])
     peak, mass, summed = merged(c_near[...], 4 * core)
     lane4 = lax.broadcasted_iota(jnp.int32, (4, 128), 1)
     row4 = lax.broadcasted_iota(jnp.int32, (4, 128), 0)
@@ -192,9 +188,8 @@
     c_far[far, 0:4, :] = summed
     c_far[far, 4:5, :] = stats
     for d in (8, 7, 9, 6, 10, 5, 11, 4, 12, 3, 13, 2, 14, 1, 15):
-        send(c_far.at[far], c_far.at[far], c_far_sem.at[far], far_id(d))
-    for d in range(1, FAR):
-        landed(c_far, lax.rem(far + d, FAR), c_far_sem)
+        send(4, c_far.at[far], c_far.at[far], recv_sem.at[3], far_id(d))
+    arrived(c_far, FAR - 1, recv_sem.at[3])
     peak, mass, summed = merged(c_far[...], 0)
     ratio = summed / mass
     lines = []
@@ -204,9 +199,8 @@
         lines.append(attended * lax.rsqrt(mean + eps) * hgain[...] * 0.8)
     nbuf[near] = jnp.concatenate(lines, axis=0).astype(BF16).astype(F32)
     for d in (4, 5, 3, 2, 6, 7, 1):
-        send(nbuf.at[near], nbuf.at[near], n_sem.at[near], near_id(d))
-    for d in range(1, NEAR):
-        landed(nbuf, lax.rem(near + d, NEAR), n_sem)
+        send(5, nbuf.at[near], nbuf.at[near], recv_sem.at[4], near_id(d))
+    arrived(nbuf, NEAR - 1, recv_sem.at[4])
     part = jnp.zeros((SEQS, 32), F32)
     for h in range(HEADS):
         head = jnp.concatenate(
@@ -219,18 +213,18 @@
     part = part.astype(BF16).astype(F32)
     pbuf[tp] = jnp.concatenate([part, jnp.zeros((SEQS, 96), F32)], axis=1)
     for d in (2, 1, 3):
-        send(pbuf.at[tp], pbuf.at[tp], p_sem.at[tp], group_id(d))
-    for d in range(1, GROUPS):
-        landed(pbuf, lax.rem(tp + d, GROUPS), p_sem)
+        send(6, pbuf.at[tp], pbuf.at[tp], recv_sem.at[5], group_id(d))
+    for phase, (buf, count) in enumerate(
+        ((a_send, NEAR), (a_far, FAR), (qbuf, NEAR), (c_send, NEAR), (c_far, FAR), (nbuf, NEAR), (pbuf, GROUPS))
+    ):
+        arrived(buf, count - 1, send_sem.at[phase])
+    arrived(pbuf, GROUPS - 1, recv_sem.at[5])
     out_ref[...] = jnp.sum(pbuf[...], axis=0)[:, 0:32].astype(BF16)
-    for copy in sends:
-        copy.wait_send()
 
 
 def body(tokens, norm_gain, query_weight, cache_keys, cache_values, lengths, lambdas, head_gain, out_weight):
     seqs, span, heads, size = cache_keys.shape
     hbm = pl.BlockSpec(memory_space=pltpu.HBM)
-    n_sends = 7 + 15 + 7 + 7 + 15 + 7 + 3
     return pl.pallas_call(
         kernel,
         name="decode",
@@ -258,14 +252,10 @@
             pltpu.VMEM((GROUPS, SEQS, 128), F32),
             pltpu.SemaphoreType.DMA((7,)),
             pltpu.SemaphoreType.DMA((2 * SEQS,)),
-            pltpu.SemaphoreType.DMA((n_sends,)),
-            pltpu.SemaphoreType.DMA((NEAR,)),
-            pltpu.SemaphoreType.DMA((FAR,)),
-            pltpu.SemaphoreType.DMA((NEAR,)),
-            pltpu.SemaphoreType.DMA((NEAR,)),
-            pltpu.SemaphoreType.DMA((FAR,)),
-            pltpu.SemaphoreType.DMA((NEAR,)),
-            pltpu.SemaphoreType.DMA((GROUPS,)),
+            pltpu.SemaphoreType.DMA((7,)),
+            pltpu.SemaphoreType.DMA((6,)),
+            pltpu.SemaphoreType.DMA((SEQS,)),
+            pltpu.SemaphoreType.REGULAR((2,)),
         ],
         compiler_params=pltpu.CompilerParams(
             collective_id=0, has_side_effects=True

time: 53.2 us -> 49.6 us (0.932)
  Pallas kernels: 51.9 us -> 48.2 us
    pallas_call x1, Pallas kernels: 51.9 us -> 48.2 us  [body(): pl.pallas_call(kernel, name='decode', out_shape=jax.ShapeDtypeStruct((seq...]
where the time goes in v2:
time: 49.6 us; the launch traced here: 49.5 us
  Pallas kernels  48.2 us (97%)
  local copies, waits for them, and re-layouts  1.24 us (2%)
    pallas_call x1, Pallas kernels, body(): pl.pallas_call(kernel, name='decode', out_shape=jax.ShapeDtypeStruct((seq...  48.2 us
    unnamed x1, local copies, waits for them, and re-layouts  1.24 us

profile of v2, /device:TPU:1, one launch (start us, length us, event | category | flops | bytes accessed | tf_op | source)
XLA Modules:
  0.0 49.5 jit_solution(5939205715354011656)
XLA Ops:
  0.0 48.2 %decode.1 = bf16[4,32]{1,0:T(4,128)(2,1)} custom-call(bf16[4,32]{1,0:T(4,128)(2,1)} %tokens_hbm.1, f32[1,32]{1,0:T(1,128)} %bitcast.8, bf16[32,512]{1,0:T(8,128)(2,1)} %wq_hbm.1, bf16[4,2048,128]{2,1,0:T(8,128)(2,1)} %bitcast.5, bf16[4,2048,128]{2,1,0:T(8,128)(2,1)} %bitcast.6, s32[4]{0:T(128)} %lengths_hbm.1, f32[4]{0:T(128)} %lambdas_hbm.1, ...), custom_call_target="tpu_custom_call" | custom-call | tf_op jit(solution)/shard_map/decode/pallas_call | solution.py:228
  48.3 1.2 %copy.11 = bf16[4,32]{1,0:T(4,128)(2,1)} copy(bf16[4,32]{1,0:T(4,128)(2,1)} %decode.1) | data formatting | bytes 512
